TPU v7x, 256 devices: a 4x2x16 block of a 4x16x16 slice. The times are simulated.
256 devices in a mesh: grp: 2 (over y), sp: 32 (over z, core), tp: 4 (over x).
Axes of the slice: x: 4, y: 2, z: 16, core: 2. Of those that a mesh axis runs over, the one named last changes fastest.
The devices are a block of a 4x16x16 slice.
Arguments:
- queries: bfloat16 [16384, 512], P(('grp', 'sp'), 'tp'), parts along dimension 0, may hold values from -6 to 6
- key_rows: bfloat16 [16384, 512], P(('grp', 'sp'), 'tp'), parts along dimension 0, may hold values from -6 to 6
- value_rows: bfloat16 [16384, 1024], P(('grp', 'sp'), 'tp'), parts along dimension 0, may hold values from -6 to 6
- out_gate: bfloat16 [16384, 1024], P(('grp', 'sp'), 'tp'), parts along dimension 0, may hold values from -6 to 6
- log_decay: float32 [2, 16384, 512], P(None, ('grp', 'sp'), 'tp'), parts along dimension 1
- doc_ids: int32 [16384], P(('grp', 'sp')), parts along dimension 0, may hold values from 0 to 3, as said below
- head_gain: float32 [1024], P('tp'), may hold values from 0.1 to 1.9
- out_weight: bfloat16 [1024, 2048], P('tp'), may hold values from -0.375 to 0.375
- residual: bfloat16 [16384, 2048], P(('grp', 'sp'), 'tp'), parts along dimension 0
- norm_gain: float32 [2, 2048], replicated, may hold values from 0.1 to 1.9
- norm_bias: float32 [2, 2048], replicated, may hold values from -3 to 3
- gate_weight: bfloat16 [2048, 3072], P('sp', 'tp'), may hold values from -0.125 to 0.125
- up_weight: bfloat16 [2048, 3072], P('sp', 'tp'), may hold values from -0.125 to 0.125
- down_weight: bfloat16 [3072, 2048], P('tp', 'sp'), may hold values from -0.109375 to 0.109375
Outputs:
- layer_out: bfloat16 [16384, 2048], P(('grp', 'sp'), 'tp'), parts along dimension 0
There are 2 independent parts, one for each index of `grp`. A program takes and returns all parts, laid end to end along the dimension named above; an argument that names none is the same for every part. Nothing has to cross between parts.
Inputs may be any that keep to these rules, and one draw needn't show every extreme that they name: `doc_ids`: document numbers start at 0 and never fall; they rise by one at each of 3 positions, the k-th rise lying within half of 256 positions of k times 8192 divided by 4.
All inputs are finite; a program needn't handle non-finite values.
Results may differ from a plain program's by a relative error of at most 0.009.
Values may be sent and summed in bfloat16 or wider, within the bound.
No kernel may reach another device: no remote copies, remote signals or barrier semaphores. Data moves between devices by JAX's collectives and lax.ppermute only.
A program may use at most 128 MiB of HBM per device.

v0:
```python
import functools
import jax
import jax.numpy as jnp
from jax import lax
from jax.experimental import pallas as pl
from jax.experimental.pallas import tpu as pltpu
from jax.sharding import PartitionSpec as P


DK = 32
DV = 64
DOCS = 4
EPS = 1e-06
META = 8
STREAM_MIB = 40
F32 = jnp.float32
BF = jnp.bfloat16


def iota(shape, dim):
    return lax.broadcasted_iota(jnp.int32, shape, dim)


def mm(a, b, dims=((1,), (0,))):
    return lax.dot_general(a, b, (dims, ((), ())), preferred_element_type=F32)


def partner(total, upper, h):
    n = total.shape[0]
    return jnp.where(upper, pltpu.roll(total, h, 0), pltpu.roll(total, n - h, 0))


def levels(g, r):
    n = g.shape[0]
    row = iota(g.shape, 0)
    zero = jnp.zeros_like(g)
    gi, gx, ri, rx, gt, rt = g, zero, r, zero, g, r
    h = 1
    while h < n:
        upper = (row & h) != 0
        yield h, jnp.where(upper, gi, ri), jnp.where(upper, rx, gx)
        gp, rp = partner(gt, upper, h), partner(rt, upper, h)
        gi = jnp.where(upper, gi + gp, gi)
        gx = jnp.where(upper, gx, gx + gp)
        ri = jnp.where(upper, ri, ri + rp)
        rx = jnp.where(upper, rx + rp, rx)
        gt, rt = gt + gp, rt + rp
        h *= 2
    yield n, (gi, gx, gt), (ri, rx, rt)


def rows_of(docs_row):
    n = docs_row.shape[1]
    return jnp.broadcast_to(docs_row, (128, n)).T


def head_block(kw, vw):
    return (iota((kw, vw), 0) // DK) == (iota((kw, vw), 1) // DV)


def state_of(keys, values):
    kw, vw = keys.shape[1], values.shape[1]
    full = mm(keys.astype(BF), values, ((0,), (0,)))
    full = jnp.where(head_block(kw, vw), full, 0.0)
    return functools.reduce(jnp.add, [full[a : a + DK] for a in range(0, kw, DK)])


def packed(state, passing, entry, leaving):
    vw = state.shape[1]
    wide = jnp.concatenate([passing] * (vw // passing.shape[1]), axis=1)
    line = iota((META, vw), 0)
    entry = jnp.concatenate([entry] * (vw // entry.shape[1]), axis=1)
    leaving = jnp.concatenate([leaving] * (vw // leaving.shape[1]), axis=1)
    meta = jnp.where(line == 0, wide, jnp.where(line == 1, entry, leaving))
    return jnp.concatenate([state, meta], axis=0)


def states_kernel(q_ref, k_ref, v_ref, d_ref, doc_ref, qf_ref, qb_ref, keep_ref, give_ref, docs_ref):
    n, _ = q_ref.shape
    docs = rows_of(doc_ref[...].astype(F32))
    docs_ref[...] = docs
    first, last = docs[0:1], docs[n - 1 : n]
    for h, fwd, bwd in levels(d_ref[0], d_ref[1]):
        if h == n:
            break
    gi, gx, gt = fwd
    ri, rx, rt = bwd
    q = q_ref[...].astype(F32) * DK ** (-0.5)
    k = k_ref[...].astype(F32)
    v = v_ref[...]
    qf_ref[...] = (q * jnp.exp(gi)).astype(BF)
    qb_ref[...] = (q * jnp.exp(ri)).astype(BF)
    through = jnp.where(first == last, 1.0, 0.0)
    ahead = packed(
        state_of(jnp.where(docs == last, k * jnp.exp(gx), 0.0), v),
        jnp.exp(gt[0:1]) * through, first, last)
    back = packed(
        state_of(jnp.where(docs == first, k * jnp.exp(rx), 0.0), v),
        jnp.exp(rt[0:1]) * through, last, first)
    low = on_low_core()
    keep_ref[...] = jnp.where(low, ahead, back).astype(BF)
    give_ref[...] = jnp.where(low, back, ahead).astype(BF)


def on_low_core():
    return lax.rem(lax.axis_index("sp"), 2) == 0


def spread(passing, vw):
    kw = passing.shape[1]
    place = (iota((DK, kw), 1) % DK) == iota((DK, kw), 0)
    picked = jnp.where(place, jnp.broadcast_to(passing, (DK, kw)), 0.0)
    return mm(picked.astype(BF), jnp.where(head_block(kw, vw), 1.0, 0.0).astype(BF))


def chained(links, kw):
    line = lambda a, j: a[DK + j : DK + j + 1]
    vw = links[0].shape[1]
    state, passing = links[-1][:DK], line(links[-1], 0)[:, :kw]
    for near, far in reversed(list(zip(links[:-1], links[1:]))):
        through = (line(near, 0) * jnp.where(line(near, 1) == line(far, 2), 1.0, 0.0))[:, :kw]
        state = near[:DK] + spread(through, vw) * state
        passing = passing * through
    return packed(state, passing, line(links[-1], 1)[:, :kw], line(links[0], 2)[:, :kw])


def pair_kernel(keep_ref, came_ref, out_ref, *, kw):
    out_ref[...] = chained([came_ref[...].astype(F32), keep_ref[...].astype(F32)], kw).astype(BF)


def entering_kernel(keep_ref, *refs, kw):
    out_ref, give_ref = refs[-2:]
    incoming = chained([ref[...].astype(F32) for ref in refs[:-2]], kw)
    out_ref[...] = incoming.astype(BF)
    give_ref[...] = chained([keep_ref[...].astype(F32), incoming], kw).astype(BF)


def local_kernel(q_ref, k_ref, v_ref, d_ref, doc_ref, gate_ref, gain_ref, out_ref, factor_ref, qe_ref, ke_ref):
    n, kw = q_ref.shape
    vw = v_ref.shape[1]
    half = n // 2
    gate = gate_ref[...].astype(F32)
    factor_ref[...] = gain_ref[...] * (gate / (1.0 + jnp.exp(-gate)))
    heads = kw // DK
    q = q_ref[...].astype(F32) * DK ** (-0.5)
    k = k_ref[...].astype(F32)
    hs = []
    for h, eq, ek in levels(d_ref[0], d_ref[1]):
        if h < n:
            qe_ref[len(hs)] = (q * jnp.exp(eq)).astype(BF)
            ke_ref[len(hs)] = (k * jnp.exp(ek)).astype(BF)
            hs.append(h)
    drow = doc_ref[...].astype(F32)
    dcol = rows_of(drow)
    v = v_ref[...]
    lane = iota((half, kw), 1) // DK
    olane = iota((half, vw), 1) // DV
    apart = iota((half, half), 0) ^ iota((half, half), 1)
    ones = jnp.where(head_block(kw, vw), 2.0, 0.0).astype(BF)
    same = mm((q * k).astype(BF), ones) * v.astype(F32)
    for t in range(2):
        mine = slice(t * half, (t + 1) * half)
        other = slice((1 - t) * half, (2 - t) * half)
        ok_in = (dcol[mine] == drow[:, mine]) & (apart != 0)
        ok_off = dcol[mine] == drow[:, other]
        acc = same[mine]
        for head in range(heads):
            own = lane == head
            score = None
            for l, h in enumerate(hs[:-1]):
                prod = mm(jnp.where(own, qe_ref[l, mine], 0), ke_ref[l, mine], ((1,), (1,)))
                score = prod if score is None else jnp.where(apart >= h, prod, score)
            off = mm(jnp.where(own, qe_ref[len(hs) - 1, mine], 0), ke_ref[len(hs) - 1, other], ((1,), (1,)))
            score = jnp.where(ok_in, score, 0.0).astype(BF)
            off = jnp.where(ok_off, off, 0.0).astype(BF)
            res = mm(score, v[mine]) + mm(off, v[other])
            acc = acc + jnp.where(olane == head, res, 0.0)
        out_ref[mine] = acc


def mix_kernel(near_ref, factor_ref, qf_ref, qb_ref, docs_ref, mine_ref, other_ref, *outs):
    _, kw = qf_ref.shape
    vw = near_ref.shape[1]
    docs = docs_ref[...]
    out = near_ref[...]
    block = head_block(kw, vw)
    mine, other, low = mine_ref[...].astype(F32), other_ref[...].astype(F32), on_low_core()
    for q_ref, link in ((qf_ref, jnp.where(low, mine, other)), (qb_ref, jnp.where(low, other, mine))):
        state, leaving = link[:DK], link[DK + 2 : DK + 3]
        wide = jnp.where(block, jnp.concatenate([state] * (kw // DK), axis=0), 0.0)
        reach = jnp.where(docs[:, :kw] == leaving[:, :kw], q_ref[...], 0)
        out = out + mm(reach, wide.astype(BF))
    square = out * out
    high = square.astype(BF)
    low = (square - high.astype(F32)).astype(BF)
    mean = jnp.where((iota((vw, vw), 0) // DV) == (iota((vw, vw), 1) // DV), 1.0 / DV, 0.0).astype(BF)
    power = mm(high, mean) + mm(low, mean)
    all_ref = outs[-1]
    all_ref[...] = (out * lax.rsqrt(power + EPS) * factor_ref[...]).astype(BF)
    for s, part in enumerate(outs[:-1]):
        part[...] = all_ref[place(s, part.shape[0])]


SDS = jax.ShapeDtypeStruct
VMEM = pl.BlockSpec(memory_space=pltpu.VMEM)
ANY = pl.BlockSpec(memory_space=pl.ANY)


def call(kernel, outs, args, scratch=(), flops=1 << 26, mib=8, far=False):
    return pl.pallas_call(
        kernel, out_shape=outs, scratch_shapes=scratch,
        in_specs=[VMEM] * (len(args) - far) + [ANY] * far,
        out_specs=jax.tree.map(lambda _: VMEM, outs),
        cost_estimate=pl.CostEstimate(flops=flops, bytes_accessed=1 << 20, transcendentals=1 << 17),
        compiler_params=pltpu.CompilerParams(vmem_limit_bytes=mib << 20),
    )(*args)


def states(q, k, v, d, doc):
    n, kw = q.shape
    vw = v.shape[1]
    outs = (SDS((n, kw), BF),) * 2 + (SDS((DK + META, vw), BF),) * 2
    return call(states_kernel, outs + (SDS((n, 128), F32),), (q, k, v, d, doc), mib=62)


def pair(keep, came, kw):
    return call(functools.partial(pair_kernel, kw=kw), SDS(keep.shape, BF), (keep, came))


def entering(keep, links, kw):
    return call(functools.partial(entering_kernel, kw=kw), (SDS(keep.shape, BF),) * 2, (keep, *links))


def local(q, k, v, d, doc, gate, gain):
    n, kw = q.shape
    vw = v.shape[1]
    scratch = (pltpu.VMEM((n.bit_length() - 1, n, kw), BF),) * 2
    return call(local_kernel, (SDS((n, vw), F32),) * 2, (q, k, v, d, doc, gate, gain), scratch, flops=1 << 29, mib=62)


def mix(near, factor, qf, qb, docs, parts, peers):
    n, vw = near.shape
    return call(mix_kernel, (SDS((n // peers, vw), BF),) * peers, (near, factor, qf, qb, docs, *parts),
                scratch=(pltpu.VMEM((n, vw), BF),), mib=62)


def place(step, width):
    peers = lax.axis_size("tp")
    number = lax.rem(lax.axis_index("tp") + step + peers, peers)
    return pl.ds(pl.multiple_of(number * width, width), width)


def layer_norm(stream, gain, bias):
    width = stream.shape[1]
    middle = jnp.sum(stream, axis=1, keepdims=True) / width
    offset = stream - middle
    spread = jnp.sum(offset * offset, axis=1, keepdims=True) / width
    return offset * lax.rsqrt(spread + EPS) * gain + bias


def settle_kernel(*refs, peers):
    mixed, weights, residual = (refs[j * peers : (j + 1) * peers] for j in range(3))
    gain_ref, bias_ref, settled_ref, features_ref, stream_ref = refs[3 * peers :]
    for s in range(peers):
        width = residual[s].shape[1]
        stream_ref[:, place(-s, width)] = residual[s][...].astype(F32)
    stream = stream_ref[...]
    for s in range(peers):
        stream = stream + mm(mixed[s][...], weights[s][...]).astype(BF).astype(F32)
    settled = layer_norm(stream, gain_ref[0:1], bias_ref[0:1])
    settled_ref[...] = settled
    features_ref[...] = settled.astype(BF)


def settle(mixed, weights, residual, gain, bias):
    peers = len(mixed)
    rows, width = mixed[0].shape[0], weights[0].shape[1]
    args = (*mixed, *weights, *residual, gain, bias)
    return call(functools.partial(settle_kernel, peers=peers), (SDS((rows, width), F32), SDS((rows, width), BF)),
                args, (pltpu.VMEM((rows, width), F32),), flops=1 << 28, mib=12)


def forward_kernel(*refs, count, hidden, cut, streams):
    pieces, w_ref, down, inner_ref = refs[:count], refs[count], refs[count + 1 : 2 * count + 1], refs[-1]
    n, full = pieces[0].shape
    steps = hidden // cut
    if streams:
        source, w_ref, inner_ref, sem = w_ref, *refs[-3:]
        spans = [(slice(0, full), slice(part * hidden + j * cut, part * hidden + (j + 1) * cut))
                 for j in range(steps) for part in range(2)]
        spans += [(slice(o, o + full // 2), slice(2 * hidden, 3 * hidden)) for o in range(0, full, full // 2)]
        copies = [pltpu.make_async_copy(source.at[span], w_ref.at[span], sem.at[k]) for k, span in enumerate(spans)]
        for copy in copies:
            copy.start()
    ready = lambda k: copies[k].wait() if streams else None
    x = jnp.concatenate([piece[...] for piece in pieces], axis=0) if count > 1 else pieces[0][...]
    for j in range(steps):
        a, b = j * cut, (j + 1) * cut
        ready(2 * j)
        gate = mm(x, w_ref[:, a:b])
        ready(2 * j + 1)
        up = mm(x, w_ref[:, hidden + a : hidden + b])
        inner_ref[:, a:b] = (gate / (1.0 + jnp.exp(-gate)) * up).astype(BF)
    for o in range(2):
        rows = slice(o * full // 2, (o + 1) * full // 2)
        ready(2 * steps + o)
        total = mm(inner_ref[...], w_ref[rows, 2 * hidden :], ((1,), (1,))).astype(BF)
        for s in range(count):
            down[s][:, rows] = total[s * n : (s + 1) * n]


def forward(pieces, weights, hidden, streams=False, cut=384):
    count = len(pieces)
    n, full = pieces[0].shape
    outs = (SDS((n, full), BF),) * count
    scratch = (pltpu.VMEM((count * n, hidden), BF),)
    if streams:
        outs += (SDS(weights.shape, BF),)
        scratch += (pltpu.SemaphoreType.DMA((2 * hidden // cut + 2,)),)
    return call(
        functools.partial(forward_kernel, count=count, hidden=hidden, cut=cut, streams=streams),
        outs, (*pieces, weights), scratch, flops=6 * count * n * full * hidden,
        mib=STREAM_MIB if streams else 8, far=streams)


def finish_kernel(settled_ref, *refs, peers):
    down = refs[:peers]
    gain_ref, bias_ref = refs[peers : peers + 2]
    outs, all_ref = refs[peers + 2 : -1], refs[-1]
    total = down[0][...].astype(F32)
    for s in range(1, peers):
        total = total + down[s][...].astype(F32)
    all_ref[...] = layer_norm(settled_ref[...] + 0.5 * total, gain_ref[1:2], bias_ref[1:2])
    for s in range(peers):
        outs[s][...] = all_ref[:, place(s, outs[s].shape[1])].astype(BF)


def finish(settled, down, gain, bias):
    peers = len(down)
    n, full = settled.shape
    return call(functools.partial(finish_kernel, peers=peers), (SDS((n, full // peers), BF),) * peers,
                (settled, *down, gain, bias), (pltpu.VMEM((n, full), F32),))


def placed_kernel(*refs):
    for s, part in enumerate(refs[:-1]):
        refs[-1][place(-s, part.shape[0])] = part[...]


def placed(parts):
    n, width = parts[0].shape
    return call(placed_kernel, SDS((len(parts) * n, width), BF), parts)


def ring(axis, step):
    peers = lax.axis_size(axis)
    return [(i, (i + step) % peers) for i in range(peers)]


def across(step):
    peers = lax.axis_size("sp")
    moves = [(i, i + 2 * step if i % 2 == 0 else i - 2 * step) for i in range(peers)]
    return [(i, j) for i, j in moves if 0 <= j < peers]


def other_core(x):
    return lax.ppermute(x, "sp", [(i, i ^ 1) for i in range(lax.axis_size("sp"))])


def carried(keep, give, kw, reach):
    whole = pair(keep, other_core(give), kw)
    links = [lax.ppermute(whole, "sp", across(step)) for step in range(1, -(-reach // 2) + 1)]
    mine, give = entering(keep, links, kw)
    return mine, other_core(give)


def from_peers(parts, axis):
    return [lax.ppermute(parts[s], axis, ring(axis, s)) for s in range(1, len(parts))]


def swapped(parts, axis):
    return [parts[0]] + from_peers(parts, axis)


def on_device(
    queries, key_rows, value_rows, out_gate, log_decay, doc_ids, head_gain, out_weight,
    residual, norm_gain, norm_bias, gate_weight, up_weight, down_weight,
):
    peers, me = lax.axis_size("tp"), lax.axis_index("tp")
    length, kw = queries.shape
    hidden = gate_weight.shape[1]
    own = length // peers
    weights = lax.all_gather(
        jnp.concatenate([gate_weight, up_weight, down_weight.T], axis=1), "sp", axis=0, tiled=True
    )
    docs = doc_ids[None]
    qf, qb, keep, give, where = states(queries, key_rows, value_rows, log_decay, docs)
    reach = -(-length * lax.axis_size("sp") // DOCS // length) + 1
    parts = carried(keep, give, kw, reach)
    out_weight, _ = lax.optimization_barrier((out_weight, give))
    out_weights = swapped([out_weight] * peers, "tp")
    near, factor = local(queries, key_rows, value_rows, log_decay, docs, out_gate, head_gain[None])
    residual, _ = lax.optimization_barrier((residual, near))
    streams = swapped(
        [lax.dynamic_slice_in_dim(residual, (me + s) % peers * own, own, 0) for s in range(peers)], "tp"
    )
    mixed = swapped(mix(near, factor, qf, qb, where, parts, peers), "tp")
    settled, features = settle(mixed, out_weights, streams, norm_gain, norm_bias)
    pieces = swapped([features] * peers, "tp")
    behind = lambda group: [pieces[-s % peers] for s in group]
    send = lambda part, s: lax.ppermute(part, "tp", ring("tp", s))
    two, one, three, weights = forward(behind([2, 1, 3]), weights, hidden, streams=True)
    two = send(two, 2)
    one, three = send(one, 1), send(three, 3)
    own_part, = forward(behind([0]), weights, hidden)
    return placed(swapped(finish(settled, [own_part, one, two, three], norm_gain, norm_bias), "tp"))


def solution(mesh):
    rows = ("grp", "sp")
    in_specs = (
        P(rows, "tp"), P(rows, "tp"), P(rows, "tp"), P(rows, "tp"), P(None, rows, "tp"),
        P(rows), P("tp"), P("tp", None), P(rows, "tp"), P(), P(),
        P("sp", "tp"), P("sp", "tp"), P("tp", "sp"),
    )
    return jax.shard_map(
        on_device, mesh=mesh, in_specs=in_specs, out_specs=P(rows, "tp"), check_vma=False
    )
```

profile of v0, /device:TPU:40, one launch (start us, length us, event | category | flops | bytes accessed | tf_op | source)
XLA Modules:
  0.0 140.4 jit_solution(9756168713683702065)
XLA Ops:
  6.6 1.7 %pad_maximum_fusion = bf16[64,2304]{1,0:T(8,128)(2,1)} fusion(bf16[64,768]{1,0:T(8,128)(2,1)} %bitcast.3, bf16[64,768]{1,0:T(8,128)(2,1)} %param.26, bf16[64,768]{1,0:T(8,128)(2,1)} %param.25), kind=kLoop, calls=%fused_computation | loop fusion | flops 884736 | bytes 589824 | tf_op jit(solution)/shard_map/concatenate | solution.py:394
  8.3 2.4 %shard_map.137 = (bf16[256,128]{1,0:T(8,128)(2,1)}, bf16[256,128]{1,0:T(8,128)(2,1)}, bf16[40,256]{1,0:T(8,128)(2,1)}, bf16[40,256]{1,0:T(8,128)(2,1)}, f32[256,128]{1,0:T(8,128)}) custom-call(bf16[256,128]{1,0:T(8,128)(2,1)} %q_ref.3, bf16[256,128]{1,0:T(8,128)(2,1)} %k_ref.3, bf16[256,256]{1,0:T(8,128)(2,1)} %v_ref.3, f32[2,256,128]{2,1,0:T(8,128)} %d_ref.3, ...), custom_call_target="tpu_custom_call" | custom-call | flops 67108864 | bytes 1048576 | tf_op jit(solution)/shard_map/pallas_call | solution.py:210
  10.7 3.2 %collective-permute-start.12 = (bf16[256,2048]{1,0:T(8,128)(2,1)}, bf16[256,2048]{1,0:T(8,128)(2,1)S(1)}, u32[]{:S(2)}, u32[]{:S(2)}) collective-permute-start(bf16[256,2048]{1,0:T(8,128)(2,1)} %refs_4_.1), channel_id=1, source_target_pairs={{0,3},{1,0},{2,1},{3,2},{4,7},{5,4},{6,5},{7,6},{8,11},{9,8},{10,9... | collective-permute-start | bytes 3145736 | tf_op jit(solution)/shard_map/ppermute | solution.py:378
  13.9 0.5 collective-permute-start.11
  14.4 1.0 collective-permute-start.10
  15.5 1.4 collective-permute-done.came_ref
  16.9 0.7 copy-done.7
  17.7 14.8 %collective-permute-start.5 = (bf16[40,256]{1,0:T(8,128)(2,1)S(1)}, bf16[40,256]{1,0:T(8,128)(2,1)S(1)}, u32[]{:S(2)}, u32[]{:S(2)}) collective-permute-start(bf16[40,256]{1,0:T(8,128)(2,1)S(1)} %shard_map.138), channel_id=1, source_target_pairs={{0,40},{8,48},{16,56},{24,64},{32,72},{40,80},{44,4},{48,88},{52,1... | collective-permute-start | bytes 61448 | tf_op jit(solution)/shard_map/ppermute | solution.py:372
  32.5 11.7 %collective-permute-start.4 = (bf16[40,256]{1,0:T(8,128)(2,1)S(1)}, bf16[40,256]{1,0:T(8,128)(2,1)S(1)}, u32[]{:S(2)}, u32[]{:S(2)}) collective-permute-start(bf16[40,256]{1,0:T(8,128)(2,1)S(1)} %shard_map.138), channel_id=1, source_target_pairs={{0,32},{8,40},{16,48},{24,56},{32,64},{36,4},{40,72},{44,12},{48,8... | collective-permute-start | bytes 61448 | tf_op jit(solution)/shard_map/ppermute | solution.py:372
  44.2 6.4 %collective-permute-start.3 = (bf16[40,256]{1,0:T(8,128)(2,1)S(1)}, bf16[40,256]{1,0:T(8,128)(2,1)S(1)}, u32[]{:S(2)}, u32[]{:S(2)}) collective-permute-start(bf16[40,256]{1,0:T(8,128)(2,1)S(1)} %shard_map.138), channel_id=1, source_target_pairs={{0,24},{8,32},{16,40},{24,48},{28,4},{32,56},{36,12},{40,64},{44,2... | collective-permute-start | bytes 61448 | tf_op jit(solution)/shard_map/ppermute | solution.py:372
  50.6 4.9 %shard_map.136 = (f32[256,256]{1,0:T(8,128)}, f32[256,256]{1,0:T(8,128)}) custom-call(bf16[256,128]{1,0:T(8,128)(2,1)} %q_ref.3, bf16[256,128]{1,0:T(8,128)(2,1)} %k_ref.3, bf16[256,256]{1,0:T(8,128)(2,1)} %v_ref.3, f32[2,256,128]{2,1,0:T(8,128)} %d_ref.3, s32[1,256]{1,0:T(1,128)} %bitcast.5, bf16[256,256]{1,0:T(8,128)(2,1)} %gate_ref.1, f32[1,256]{1,0:T(1,128)} %bitcast.6), custom_call_target="tpu_custom_call" | custom-call | flops 536870912 | bytes 1048576 | tf_op jit(solution)/shard_map/pallas_call | solution.py:210
  55.5 5.1 %collective-permute-start.2 = (bf16[40,256]{1,0:T(8,128)(2,1)S(1)}, bf16[40,256]{1,0:T(8,128)(2,1)S(1)}, u32[]{:S(2)}, u32[]{:S(2)}) collective-permute-start(bf16[40,256]{1,0:T(8,128)(2,1)S(1)} %shard_map.138), channel_id=1, source_target_pairs={{0,16},{8,24},{16,32},{20,4},{24,40},{28,12},{32,48},{36,20},{40,5... | collective-permute-start | bytes 61448 | tf_op jit(solution)/shard_map/ppermute | solution.py:372
  60.7 3.8 %collective-permute-start.1 = (bf16[40,256]{1,0:T(8,128)(2,1)S(1)}, bf16[40,256]{1,0:T(8,128)(2,1)S(1)}, u32[]{:S(2)}, u32[]{:S(2)}) collective-permute-start(bf16[40,256]{1,0:T(8,128)(2,1)S(1)} %shard_map.138), channel_id=1, source_target_pairs={{0,8},{8,16},{12,4},{16,24},{20,12},{24,32},{28,20},{32,40},{36,28... | collective-permute-start | bytes 61448 | tf_op jit(solution)/shard_map/ppermute | solution.py:372
  64.5 1.0 constant_dynamic-slice_fusion
  65.5 2.3 %collective-permute-start.15 = (bf16[64,512]{1,0:T(8,128)(2,1)S(1)}, bf16[64,512]{1,0:T(8,128)(2,1)S(1)}, u32[]{:S(2)}, u32[]{:S(2)}) collective-permute-start(bf16[64,512]{1,0:T(8,128)(2,1)S(1)} %get-tuple-element.55), channel_id=1, source_target_pairs={{0,3},{1,0},{2,1},{3,2},{4,7},{5,4},{6,5},{7,6},{8,11},{9,8},{10,9... | collective-permute-start | bytes 196616 | tf_op jit(solution)/shard_map/ppermute | solution.py:378
  67.8 0.7 copy-done.8
  68.6 0.2 shard_map.139
  68.8 0.6 copy-done.6
  69.4 1.2 collective-permute-done.6.other_ref
  70.6 1.8 %collective-permute-start.14 = (bf16[64,512]{1,0:T(8,128)(2,1)S(1)}, bf16[64,512]{1,0:T(8,128)(2,1)S(1)}, u32[]{:S(2)}, u32[]{:S(2)}) collective-permute-start(bf16[64,512]{1,0:T(8,128)(2,1)S(1)} %get-tuple-element.56), channel_id=1, source_target_pairs={{0,2},{1,3},{2,0},{3,1},{4,6},{5,7},{6,4},{7,5},{8,10},{9,11},{10,... | collective-permute-start | bytes 196616 | tf_op jit(solution)/shard_map/ppermute | solution.py:378
  72.4 2.3 %shard_map.140 = (bf16[64,256]{1,0:T(8,128)(2,1)}, bf16[64,256]{1,0:T(8,128)(2,1)}, bf16[64,256]{1,0:T(8,128)(2,1)}, bf16[64,256]{1,0:T(8,128)(2,1)}) custom-call(f32[256,256]{1,0:T(8,128)} %get-tuple-element.30.near_ref, f32[256,256]{1,0:T(8,128)} %get-tuple-element.31.factor_ref, bf16[256,128]{1,0:T(8,128)(2,1)} %get-tuple-element.32.qf_ref, ...), custom_call_target="tpu_custom_call" | custom-call | flops 67108864 | bytes 1048576 | tf_op jit(solution)/shard_map/pallas_call | solution.py:210
  74.7 2.4 %collective-permute-done.14.refs_10_ = bf16[64,512]{1,0:T(8,128)(2,1)S(1)} collective-permute-done((bf16[64,512]{1,0:T(8,128)(2,1)S(1)}, bf16[64,512]{1,0:T(8,128)(2,1)S(1)}, u32[]{:S(2)}, u32[]{:S(2)}) %collective-permute-start.14) | collective-permute-done | bytes 65568 | tf_op jit(solution)/shard_map/ppermute | solution.py:378
  77.0 0.9 collective-permute-done.13.refs_9_
  77.9 1.5 %collective-permute-start.8 = (bf16[64,256]{1,0:T(8,128)(2,1)}, bf16[64,256]{1,0:T(8,128)(2,1)S(1)}, u32[]{:S(2)}, u32[]{:S(2)}) collective-permute-start(bf16[64,256]{1,0:T(8,128)(2,1)} %get-tuple-element.41), channel_id=1, source_target_pairs={{0,2},{1,3},{2,0},{3,1},{4,6},{5,7},{6,4},{7,5},{8,10},{9,11},{10,... | collective-permute-start | bytes 98312 | tf_op jit(solution)/shard_map/ppermute | solution.py:378
  79.5 3.0 %collective-permute-done.7.refs_1_ = bf16[64,256]{1,0:T(8,128)(2,1)S(1)} collective-permute-done((bf16[64,256]{1,0:T(8,128)(2,1)}, bf16[64,256]{1,0:T(8,128)(2,1)S(1)}, u32[]{:S(2)}, u32[]{:S(2)}) %collective-permute-start.7) | collective-permute-done | bytes 32800 | tf_op jit(solution)/shard_map/ppermute | solution.py:378
  82.5 1.1 collective-permute-done.8.refs_2_
  83.6 3.0 %collective-permute-done.9.refs_3_ = bf16[64,256]{1,0:T(8,128)(2,1)S(1)} collective-permute-done((bf16[64,256]{1,0:T(8,128)(2,1)}, bf16[64,256]{1,0:T(8,128)(2,1)S(1)}, u32[]{:S(2)}, u32[]{:S(2)}) %collective-permute-start.9) | collective-permute-done | bytes 32800 | tf_op jit(solution)/shard_map/ppermute | solution.py:378
  86.6 1.2 copy-done
  87.9 0.7 copy-done.1
  88.6 0.7 copy-done.3
  89.3 0.8 copy-done.5
  90.1 2.7 %shard_map.141 = (f32[64,2048]{1,0:T(8,128)S(1)}, bf16[64,2048]{1,0:T(8,128)(2,1)S(1)}) custom-call(bf16[64,256]{1,0:T(8,128)(2,1)S(1)} %copy-done.5, bf16[64,256]{1,0:T(8,128)(2,1)S(1)} %collective-permute-done.7.refs_1_, bf16[64,256]{1,0:T(8,128)(2,1)S(1)} %collective-permute-done.8.refs_2_, bf16[64,256]{1,0:T(8,128)(2,1)S(1)} %collective-permute-done.9.refs_3_, ...), custom_call_target="tpu_custom_call" | custom-call | flops 268435456 | bytes 1048576 | tf_op jit(solution)/shard_map/pallas_call | solution.py:210
  92.9 3.2 %collective-permute-start.17 = (bf16[64,2048]{1,0:T(8,128)(2,1)S(1)}, bf16[64,2048]{1,0:T(8,128)(2,1)S(1)}, u32[]{:S(2)}, u32[]{:S(2)}) collective-permute-start(bf16[64,2048]{1,0:T(8,128)(2,1)S(1)} %get-tuple-element.46.refs_0_), channel_id=1, source_target_pairs={{0,3},{1,0},{2,1},{3,2},{4,7},{5,4},{6,5},{7,6},{8,11},{9,8},{10,9... | collective-permute-start | bytes 786440 | tf_op jit(solution)/shard_map/ppermute | solution.py:378
  96.1 9.3 %collective-permute-done.18.refs_2_ = bf16[64,2048]{1,0:T(8,128)(2,1)S(1)} collective-permute-done((bf16[64,2048]{1,0:T(8,128)(2,1)S(1)}, bf16[64,2048]{1,0:T(8,128)(2,1)S(1)}, u32[]{:S(2)}, u32[]{:S(2)}) %collective-permute-start.18) | collective-permute-done | bytes 262176 | tf_op jit(solution)/shard_map/ppermute | solution.py:378
  105.5 5.1 %shard_map.142 = (bf16[64,2048]{1,0:T(8,128)(2,1)S(1)}, bf16[64,2048]{1,0:T(8,128)(2,1)S(1)}, bf16[64,2048]{1,0:T(8,128)(2,1)S(1)}, bf16[2048,2304]{1,0:T(8,128)(2,1)S(1)}) custom-call(bf16[64,2048]{1,0:T(8,128)(2,1)S(1)} %collective-permute-done.16.refs_0_, bf16[64,2048]{1,0:T(8,128)(2,1)S(1)} %collective-permute-done.17.refs_1_, ...), custom_call_target="tpu_custom_call" | custom-call | flops 1811939328 | bytes 1048576 | tf_op jit(solution)/shard_map/pallas_call | solution.py:210
  110.5 0.9 collective-permute-start.19
  111.5 3.1 %collective-permute-start.20 = (bf16[64,2048]{1,0:T(8,128)(2,1)S(1)}, bf16[64,2048]{1,0:T(8,128)(2,1)S(1)}, u32[]{:S(2)}, u32[]{:S(2)}) collective-permute-start(bf16[64,2048]{1,0:T(8,128)(2,1)S(1)} %get-tuple-element.49), channel_id=1, source_target_pairs={{0,2},{1,3},{2,0},{3,1},{4,6},{5,7},{6,4},{7,5},{8,10},{9,11},{10,... | collective-permute-start | bytes 786440 | tf_op jit(solution)/shard_map/ppermute | solution.py:411
  114.6 2.1 %shard_map.143.refs_0_ = bf16[64,2048]{1,0:T(8,128)(2,1)S(1)} custom-call(bf16[64,2048]{1,0:T(8,128)(2,1)S(1)} %get-tuple-element.46.refs_0_, bf16[2048,2304]{1,0:T(8,128)(2,1)S(1)} %get-tuple-element.47.refs_1_), custom_call_target="tpu_custom_call" | custom-call | flops 603979776 | bytes 1048576 | tf_op jit(solution)/shard_map/pallas_call | solution.py:210
  116.7 4.2 %collective-permute-done.19.refs_1_ = bf16[64,2048]{1,0:T(8,128)(2,1)S(1)} collective-permute-done((bf16[64,2048]{1,0:T(8,128)(2,1)S(1)}, bf16[64,2048]{1,0:T(8,128)(2,1)S(1)}, u32[]{:S(2)}, u32[]{:S(2)}) %collective-permute-start.19) | collective-permute-done | bytes 262176 | tf_op jit(solution)/shard_map/ppermute | solution.py:411
  120.9 2.8 %collective-permute-done.20.refs_2_ = bf16[64,2048]{1,0:T(8,128)(2,1)S(1)} collective-permute-done((bf16[64,2048]{1,0:T(8,128)(2,1)S(1)}, bf16[64,2048]{1,0:T(8,128)(2,1)S(1)}, u32[]{:S(2)}, u32[]{:S(2)}) %collective-permute-start.20) | collective-permute-done | bytes 262176 | tf_op jit(solution)/shard_map/ppermute | solution.py:411
  123.9 0.4 shard_map.144
  124.3 1.9 %collective-permute-start.22 = (bf16[64,512]{1,0:T(8,128)(2,1)S(1)}, bf16[64,512]{1,0:T(8,128)(2,1)S(1)}, u32[]{:S(2)}, u32[]{:S(2)}) collective-permute-start(bf16[64,512]{1,0:T(8,128)(2,1)S(1)} %get-tuple-element.52), channel_id=1, source_target_pairs={{0,1},{1,2},{2,3},{3,0},{4,5},{5,6},{6,7},{7,4},{8,9},{9,10},{10,1... | collective-permute-start | bytes 196616 | tf_op jit(solution)/shard_map/ppermute | solution.py:378
  126.2 2.4 %collective-permute-start.23 = (bf16[64,512]{1,0:T(8,128)(2,1)S(1)}, bf16[64,512]{1,0:T(8,128)(2,1)S(1)}, u32[]{:S(2)}, u32[]{:S(2)}) collective-permute-start(bf16[64,512]{1,0:T(8,128)(2,1)S(1)} %get-tuple-element.53), channel_id=1, source_target_pairs={{0,2},{1,3},{2,0},{3,1},{4,6},{5,7},{6,4},{7,5},{8,10},{9,11},{10,... | collective-permute-start | bytes 196616 | tf_op jit(solution)/shard_map/ppermute | solution.py:378
  128.5 1.4 collective-permute-start.24
  129.9 0.6 collective-permute-done.22.refs_1_
  130.6 1.3 collective-permute-done.23.refs_2_
  131.9 0.9 collective-permute-done.24.refs_3_
  132.8 0.7 shard_map.145
  (37 shorter events, 0.6 us)
Async XLA Ops:
  6.5 98.9 %all-gather.2.cloned.1.call-start = ((), (), s32[]{:S(2)}) async-start(), calls=%async_computation | async-start | bytes 9732096 | tf_op jit(solution)/shard_map/all_gather | solution.py:393
  10.7 75.9 %collective-permute-start.12 = (bf16[256,2048]{1,0:T(8,128)(2,1)}, bf16[256,2048]{1,0:T(8,128)(2,1)S(1)}, u32[]{:S(2)}, u32[]{:S(2)}) collective-permute-start(bf16[256,2048]{1,0:T(8,128)(2,1)} %refs_4_.1), channel_id=1, source_target_pairs={{0,3},{1,0},{2,1},{3,2},{4,7},{5,4},{6,5},{7,6},{8,11},{9,8},{10,9... | collective-permute-start | bytes 3145736 | tf_op jit(solution)/shard_map/ppermute | solution.py:378
  13.9 72.7 %collective-permute-start.11 = (bf16[256,2048]{1,0:T(8,128)(2,1)}, bf16[256,2048]{1,0:T(8,128)(2,1)}, u32[]{:S(2)}, u32[]{:S(2)}) collective-permute-start(bf16[256,2048]{1,0:T(8,128)(2,1)} %refs_4_.1), channel_id=1, source_target_pairs={{0,2},{1,3},{2,0},{3,1},{4,6},{5,7},{6,4},{7,5},{8,10},{9,11},{10,... | collective-permute-start | bytes 3145736 | tf_op jit(solution)/shard_map/ppermute | solution.py:378
  14.4 72.2 %collective-permute-start.10 = (bf16[256,2048]{1,0:T(8,128)(2,1)}, bf16[256,2048]{1,0:T(8,128)(2,1)}, u32[]{:S(2)}, u32[]{:S(2)}) collective-permute-start(bf16[256,2048]{1,0:T(8,128)(2,1)} %refs_4_.1), channel_id=1, source_target_pairs={{0,1},{1,2},{2,3},{3,0},{4,5},{5,6},{6,7},{7,4},{8,9},{9,10},{10,1... | collective-permute-start | bytes 3145736 | tf_op jit(solution)/shard_map/ppermute | solution.py:378
  15.5 1.4 collective-permute-start
  16.9 0.7 copy-start.7
  17.7 26.4 %collective-permute-start.5 = (bf16[40,256]{1,0:T(8,128)(2,1)S(1)}, bf16[40,256]{1,0:T(8,128)(2,1)S(1)}, u32[]{:S(2)}, u32[]{:S(2)}) collective-permute-start(bf16[40,256]{1,0:T(8,128)(2,1)S(1)} %shard_map.138), channel_id=1, source_target_pairs={{0,40},{8,48},{16,56},{24,64},{32,72},{40,80},{44,4},{48,88},{52,1... | collective-permute-start | bytes 61448 | tf_op jit(solution)/shard_map/ppermute | solution.py:372
  32.5 23.0 %collective-permute-start.4 = (bf16[40,256]{1,0:T(8,128)(2,1)S(1)}, bf16[40,256]{1,0:T(8,128)(2,1)S(1)}, u32[]{:S(2)}, u32[]{:S(2)}) collective-permute-start(bf16[40,256]{1,0:T(8,128)(2,1)S(1)} %shard_map.138), channel_id=1, source_target_pairs={{0,32},{8,40},{16,48},{24,56},{32,64},{36,4},{40,72},{44,12},{48,8... | collective-permute-start | bytes 61448 | tf_op jit(solution)/shard_map/ppermute | solution.py:372
  44.2 16.5 %collective-permute-start.3 = (bf16[40,256]{1,0:T(8,128)(2,1)S(1)}, bf16[40,256]{1,0:T(8,128)(2,1)S(1)}, u32[]{:S(2)}, u32[]{:S(2)}) collective-permute-start(bf16[40,256]{1,0:T(8,128)(2,1)S(1)} %shard_map.138), channel_id=1, source_target_pairs={{0,24},{8,32},{16,40},{24,48},{28,4},{32,56},{36,12},{40,64},{44,2... | collective-permute-start | bytes 61448 | tf_op jit(solution)/shard_map/ppermute | solution.py:372
  55.5 9.9 %collective-permute-start.2 = (bf16[40,256]{1,0:T(8,128)(2,1)S(1)}, bf16[40,256]{1,0:T(8,128)(2,1)S(1)}, u32[]{:S(2)}, u32[]{:S(2)}) collective-permute-start(bf16[40,256]{1,0:T(8,128)(2,1)S(1)} %shard_map.138), channel_id=1, source_target_pairs={{0,16},{8,24},{16,32},{20,4},{24,40},{28,12},{32,48},{36,20},{40,5... | collective-permute-start | bytes 61448 | tf_op jit(solution)/shard_map/ppermute | solution.py:372
  60.7 7.1 %collective-permute-start.1 = (bf16[40,256]{1,0:T(8,128)(2,1)S(1)}, bf16[40,256]{1,0:T(8,128)(2,1)S(1)}, u32[]{:S(2)}, u32[]{:S(2)}) collective-permute-start(bf16[40,256]{1,0:T(8,128)(2,1)S(1)} %shard_map.138), channel_id=1, source_target_pairs={{0,8},{8,16},{12,4},{16,24},{20,12},{24,32},{28,20},{32,40},{36,28... | collective-permute-start | bytes 61448 | tf_op jit(solution)/shard_map/ppermute | solution.py:372
  65.5 6.9 %collective-permute-start.15 = (bf16[64,512]{1,0:T(8,128)(2,1)S(1)}, bf16[64,512]{1,0:T(8,128)(2,1)S(1)}, u32[]{:S(2)}, u32[]{:S(2)}) collective-permute-start(bf16[64,512]{1,0:T(8,128)(2,1)S(1)} %get-tuple-element.55), channel_id=1, source_target_pairs={{0,3},{1,0},{2,1},{3,2},{4,7},{5,4},{6,5},{7,6},{8,11},{9,8},{10,9... | collective-permute-start | bytes 196616 | tf_op jit(solution)/shard_map/ppermute | solution.py:378
  67.8 0.7 copy-start.8
  68.7 0.6 copy-start.6
  69.3 1.2 collective-permute-start.6
  70.6 1.8 %copy-start.9 = (bf16[40,256]{1,0:T(8,128)(2,1)}, bf16[40,256]{1,0:T(8,128)(2,1)S(1)}, u32[]{:S(2)}) copy-start(bf16[40,256]{1,0:T(8,128)(2,1)S(1)} %collective-permute-done.6.other_ref) | copy-start | bytes 61444
  70.6 6.5 %collective-permute-start.14 = (bf16[64,512]{1,0:T(8,128)(2,1)S(1)}, bf16[64,512]{1,0:T(8,128)(2,1)S(1)}, u32[]{:S(2)}, u32[]{:S(2)}) collective-permute-start(bf16[64,512]{1,0:T(8,128)(2,1)S(1)} %get-tuple-element.56), channel_id=1, source_target_pairs={{0,2},{1,3},{2,0},{3,1},{4,6},{5,7},{6,4},{7,5},{8,10},{9,11},{10,... | collective-permute-start | bytes 196616 | tf_op jit(solution)/shard_map/ppermute | solution.py:378
  72.3 5.6 %collective-permute-start.13 = (bf16[64,512]{1,0:T(8,128)(2,1)S(1)}, bf16[64,512]{1,0:T(8,128)(2,1)S(1)}, u32[]{:S(2)}, u32[]{:S(2)}) collective-permute-start(bf16[64,512]{1,0:T(8,128)(2,1)S(1)} %get-tuple-element.57), channel_id=1, source_target_pairs={{0,1},{1,2},{2,3},{3,0},{4,5},{5,6},{6,7},{7,4},{8,9},{9,10},{10,1... | collective-permute-start | bytes 196616 | tf_op jit(solution)/shard_map/ppermute | solution.py:378
  77.0 5.5 %collective-permute-start.7 = (bf16[64,256]{1,0:T(8,128)(2,1)}, bf16[64,256]{1,0:T(8,128)(2,1)S(1)}, u32[]{:S(2)}, u32[]{:S(2)}) collective-permute-start(bf16[64,256]{1,0:T(8,128)(2,1)} %get-tuple-element.40), channel_id=1, source_target_pairs={{0,1},{1,2},{2,3},{3,0},{4,5},{5,6},{6,7},{7,4},{8,9},{9,10},{10,1... | collective-permute-start | bytes 98312 | tf_op jit(solution)/shard_map/ppermute | solution.py:378
  77.9 5.6 %collective-permute-start.8 = (bf16[64,256]{1,0:T(8,128)(2,1)}, bf16[64,256]{1,0:T(8,128)(2,1)S(1)}, u32[]{:S(2)}, u32[]{:S(2)}) collective-permute-start(bf16[64,256]{1,0:T(8,128)(2,1)} %get-tuple-element.41), channel_id=1, source_target_pairs={{0,2},{1,3},{2,0},{3,1},{4,6},{5,7},{6,4},{7,5},{8,10},{9,11},{10,... | collective-permute-start | bytes 98312 | tf_op jit(solution)/shard_map/ppermute | solution.py:378
  82.5 4.1 %collective-permute-start.9 = (bf16[64,256]{1,0:T(8,128)(2,1)}, bf16[64,256]{1,0:T(8,128)(2,1)S(1)}, u32[]{:S(2)}, u32[]{:S(2)}) collective-permute-start(bf16[64,256]{1,0:T(8,128)(2,1)} %get-tuple-element.42), channel_id=1, source_target_pairs={{0,3},{1,0},{2,1},{3,2},{4,7},{5,4},{6,5},{7,6},{8,11},{9,8},{10,9... | collective-permute-start | bytes 98312 | tf_op jit(solution)/shard_map/ppermute | solution.py:378
  86.6 1.3 copy-start
  87.9 0.7 copy-start.1
  88.6 0.7 copy-start.3
  89.3 0.8 copy-start.5
  92.7 31.1 %copy-start.2 = (f32[2,2048]{1,0:T(2,128)S(1)}, f32[2,2048]{1,0:T(2,128)}, u32[]{:S(2)}) copy-start(f32[2,2048]{1,0:T(2,128)} %refs_4_.2) | copy-start | bytes 49156
  92.8 31.1 %copy-start.4 = (f32[2,2048]{1,0:T(2,128)S(1)}, f32[2,2048]{1,0:T(2,128)}, u32[]{:S(2)}) copy-start(f32[2,2048]{1,0:T(2,128)} %refs_5_.1) | copy-start | bytes 49156
  92.8 12.7 %collective-permute-start.18 = (bf16[64,2048]{1,0:T(8,128)(2,1)S(1)}, bf16[64,2048]{1,0:T(8,128)(2,1)S(1)}, u32[]{:S(2)}, u32[]{:S(2)}) collective-permute-start(bf16[64,2048]{1,0:T(8,128)(2,1)S(1)} %get-tuple-element.46.refs_0_), channel_id=1, source_target_pairs={{0,1},{1,2},{2,3},{3,0},{4,5},{5,6},{6,7},{7,4},{8,9},{9,10},{10,1... | collective-permute-start | bytes 786440 | tf_op jit(solution)/shard_map/ppermute | solution.py:378
  92.9 12.5 %collective-permute-start.17 = (bf16[64,2048]{1,0:T(8,128)(2,1)S(1)}, bf16[64,2048]{1,0:T(8,128)(2,1)S(1)}, u32[]{:S(2)}, u32[]{:S(2)}) collective-permute-start(bf16[64,2048]{1,0:T(8,128)(2,1)S(1)} %get-tuple-element.46.refs_0_), channel_id=1, source_target_pairs={{0,3},{1,0},{2,1},{3,2},{4,7},{5,4},{6,5},{7,6},{8,11},{9,8},{10,9... | collective-permute-start | bytes 786440 | tf_op jit(solution)/shard_map/ppermute | solution.py:378
  96.1 9.3 %collective-permute-start.16 = (bf16[64,2048]{1,0:T(8,128)(2,1)S(1)}, bf16[64,2048]{1,0:T(8,128)(2,1)S(1)}, u32[]{:S(2)}, u32[]{:S(2)}) collective-permute-start(bf16[64,2048]{1,0:T(8,128)(2,1)S(1)} %get-tuple-element.46.refs_0_), channel_id=1, source_target_pairs={{0,2},{1,3},{2,0},{3,1},{4,6},{5,7},{6,4},{7,5},{8,10},{9,11},{10,... | collective-permute-start | bytes 786440 | tf_op jit(solution)/shard_map/ppermute | solution.py:378
  110.5 10.4 %collective-permute-start.19 = (bf16[64,2048]{1,0:T(8,128)(2,1)S(1)}, bf16[64,2048]{1,0:T(8,128)(2,1)S(1)}, u32[]{:S(2)}, u32[]{:S(2)}) collective-permute-start(bf16[64,2048]{1,0:T(8,128)(2,1)S(1)} %get-tuple-element.48), channel_id=1, source_target_pairs={{0,1},{1,2},{2,3},{3,0},{4,5},{5,6},{6,7},{7,4},{8,9},{9,10},{10,1... | collective-permute-start | bytes 786440 | tf_op jit(solution)/shard_map/ppermute | solution.py:411
  111.5 12.2 %collective-permute-start.20 = (bf16[64,2048]{1,0:T(8,128)(2,1)S(1)}, bf16[64,2048]{1,0:T(8,128)(2,1)S(1)}, u32[]{:S(2)}, u32[]{:S(2)}) collective-permute-start(bf16[64,2048]{1,0:T(8,128)(2,1)S(1)} %get-tuple-element.49), channel_id=1, source_target_pairs={{0,2},{1,3},{2,0},{3,1},{4,6},{5,7},{6,4},{7,5},{8,10},{9,11},{10,... | collective-permute-start | bytes 786440 | tf_op jit(solution)/shard_map/ppermute | solution.py:411
  114.6 9.3 %collective-permute-start.21 = (bf16[64,2048]{1,0:T(8,128)(2,1)S(1)}, bf16[64,2048]{1,0:T(8,128)(2,1)S(1)}, u32[]{:S(2)}, u32[]{:S(2)}) collective-permute-start(bf16[64,2048]{1,0:T(8,128)(2,1)S(1)} %get-tuple-element.50), channel_id=1, source_target_pairs={{0,3},{1,0},{2,1},{3,2},{4,7},{5,4},{6,5},{7,6},{8,11},{9,8},{10,9... | collective-permute-start | bytes 786440 | tf_op jit(solution)/shard_map/ppermute | solution.py:411
  124.3 6.3 %collective-permute-start.22 = (bf16[64,512]{1,0:T(8,128)(2,1)S(1)}, bf16[64,512]{1,0:T(8,128)(2,1)S(1)}, u32[]{:S(2)}, u32[]{:S(2)}) collective-permute-start(bf16[64,512]{1,0:T(8,128)(2,1)S(1)} %get-tuple-element.52), channel_id=1, source_target_pairs={{0,1},{1,2},{2,3},{3,0},{4,5},{5,6},{6,7},{7,4},{8,9},{9,10},{10,1... | collective-permute-start | bytes 196616 | tf_op jit(solution)/shard_map/ppermute | solution.py:378
  126.2 5.8 %collective-permute-start.23 = (bf16[64,512]{1,0:T(8,128)(2,1)S(1)}, bf16[64,512]{1,0:T(8,128)(2,1)S(1)}, u32[]{:S(2)}, u32[]{:S(2)}) collective-permute-start(bf16[64,512]{1,0:T(8,128)(2,1)S(1)} %get-tuple-element.53), channel_id=1, source_target_pairs={{0,2},{1,3},{2,0},{3,1},{4,6},{5,7},{6,4},{7,5},{8,10},{9,11},{10,... | collective-permute-start | bytes 196616 | tf_op jit(solution)/shard_map/ppermute | solution.py:378
  128.5 4.3 %collective-permute-start.24 = (bf16[64,512]{1,0:T(8,128)(2,1)S(1)}, bf16[64,512]{1,0:T(8,128)(2,1)S(1)}, u32[]{:S(2)}, u32[]{:S(2)}) collective-permute-start(bf16[64,512]{1,0:T(8,128)(2,1)S(1)} %get-tuple-element.54), channel_id=1, source_target_pairs={{0,3},{1,0},{2,1},{3,2},{4,7},{5,4},{6,5},{7,6},{8,11},{9,8},{10,9... | collective-permute-start | bytes 196616 | tf_op jit(solution)/shard_map/ppermute | solution.py:378
Sparse Core Ops, SparseCore 0:
  9.2 93.5 all-gather.1
where the time goes:
time: 141 us; the launch traced here: 140 us
  starting transfers between devices  65.2 us (46%)
  waiting for transfers between devices  32.5 us (23%)
  Pallas kernels  20.9 us (15%)
  between operations  13.6 us (10%)
  local copies, waits for them, and re-layouts  6.49 us (5%)
  other arithmetic  1.73 us (1%)
    ppermute x5, starting transfers between devices, carried(): lax.ppermute(whole, 'sp', across(step))  41.8 us
    ppermute x15, waiting for transfers between devices, from_peers(): lax.ppermute(parts[s], axis, ring(axis, s))  22.6 us
    pallas_call x10, Pallas kernels, call(): pl.pallas_call(kernel, out_shape=outs, scratch_shapes=scratch, in_specs=[...  20.9 us
    ppermute x15, starting transfers between devices, from_peers(): lax.ppermute(parts[s], axis, ring(axis, s))  19.4 us
    ppermute x3, waiting for transfers between devices, on_device(): send = lambda part, s: lax.ppermute(part, 'tp', ring('tp', s))  7.23 us
    unnamed x20, local copies, waits for them, and re-layouts  5.52 us
    ppermute x3, starting transfers between devices, on_device(): send = lambda part, s: lax.ppermute(part, 'tp', ring('tp', s))  4.03 us
  transfers between devices with their start and end apart: 26, of which 14 were waited for; matrix products, arithmetic and copies ran while one was open for 1% of the time, Pallas kernels for 10%

commit v1 on v0

--- a/solution.py
+++ b/solution.py
@@ -358,9 +358,12 @@
 
 
 def across(step):
-    peers = lax.axis_size("sp")
-    moves = [(i, i + 2 * step if i % 2 == 0 else i - 2 * step) for i in range(peers)]
-    return [(i, j) for i, j in moves if 0 <= j < peers]
+    chips = lax.axis_size("sp") // 2
+    span = chips // DOCS
+    reach = lambda behind: behind + 1 if behind else span + 1
+    up = [(2 * (chip - step), 2 * chip) for chip in range(step, chips) if step <= reach(chip % span)]
+    down = [(2 * (chip + step) + 1, 2 * chip + 1) for chip in range(chips - step) if step <= reach(span - 1 - chip % span)]
+    return up + down
 
 
 def other_core(x):

time: 141 us -> 140 us (level)
  starting transfers between devices: 65.2 us -> 62.1 us
  waiting for transfers between devices: 32.5 us -> 34.3 us
    ppermute x5, starting transfers between devices: 41.8 us -> 37.3 us  [carried(): lax.ppermute(whole, 'sp', across(step))]
    ppermute x3, starting transfers between devices: 4.03 us -> 5.51 us  [on_device(): send = lambda part, s: lax.ppermute(part, 'tp', ring('tp', s))]
  transfers between devices with their start and end apart: 26 -> 26, of which waited for: 14 -> 14; matrix products, arithmetic and copies ran while one was open for 1% -> 1% of each run, Pallas kernels for 10% -> 11%
where the time goes in v1:
time: 140 us; the launch traced here: 139 us
  starting transfers between devices  62.1 us (44%)
  waiting for transfers between devices  34.3 us (24%)
  Pallas kernels  20.9 us (15%)
  between operations  13.6 us (10%)
  local copies, waits for them, and re-layouts  6.49 us (5%)
  other arithmetic  1.73 us (1%)
    ppermute x5, starting transfers between devices, carried(): lax.ppermute(whole, 'sp', across(step))  37.3 us
    ppermute x15, waiting for transfers between devices, from_peers(): lax.ppermute(parts[s], axis, ring(axis, s))  22.6 us
    pallas_call x10, Pallas kernels, call(): pl.pallas_call(kernel, out_shape=outs, scratch_shapes=scratch, in_specs=[...  20.9 us
    ppermute x15, starting transfers between devices, from_peers(): lax.ppermute(parts[s], axis, ring(axis, s))  19.3 us
    ppermute x3, waiting for transfers between devices, on_device(): send = lambda part, s: lax.ppermute(part, 'tp', ring('tp', s))  8.41 us
    unnamed x20, local copies, waits for them, and re-layouts  5.52 us
    ppermute x3, starting transfers between devices, on_device(): send = lambda part, s: lax.ppermute(part, 'tp', ring('tp', s))  5.51 us
  transfers between devices with their start and end apart: 26, of which 14 were waited for; matrix products, arithmetic and copies ran while one was open for 1% of the time, Pallas kernels for 11%

profile of v1, /device:TPU:40, one launch (start us, length us, event | category | flops | bytes accessed | tf_op | source)
XLA Modules:
  0.0 139.1 jit_solution(5780687108358289763)
XLA Ops:
  6.6 1.7 %pad_maximum_fusion = bf16[64,2304]{1,0:T(8,128)(2,1)} fusion(bf16[64,768]{1,0:T(8,128)(2,1)} %bitcast.3, bf16[64,768]{1,0:T(8,128)(2,1)} %param.26, bf16[64,768]{1,0:T(8,128)(2,1)} %param.25), kind=kLoop, calls=%fused_computation | loop fusion | flops 884736 | bytes 589824 | tf_op jit(solution)/shard_map/concatenate | solution.py:397
  8.3 2.4 %shard_map.137 = (bf16[256,128]{1,0:T(8,128)(2,1)}, bf16[256,128]{1,0:T(8,128)(2,1)}, bf16[40,256]{1,0:T(8,128)(2,1)}, bf16[40,256]{1,0:T(8,128)(2,1)}, f32[256,128]{1,0:T(8,128)}) custom-call(bf16[256,128]{1,0:T(8,128)(2,1)} %q_ref.3, bf16[256,128]{1,0:T(8,128)(2,1)} %k_ref.3, bf16[256,256]{1,0:T(8,128)(2,1)} %v_ref.3, f32[2,256,128]{2,1,0:T(8,128)} %d_ref.3, ...), custom_call_target="tpu_custom_call" | custom-call | flops 67108864 | bytes 1048576 | tf_op jit(solution)/shard_map/pallas_call | solution.py:210
  10.7 3.2 %collective-permute-start.12 = (bf16[256,2048]{1,0:T(8,128)(2,1)}, bf16[256,2048]{1,0:T(8,128)(2,1)S(1)}, u32[]{:S(2)}, u32[]{:S(2)}) collective-permute-start(bf16[256,2048]{1,0:T(8,128)(2,1)} %refs_4_.1), channel_id=1, source_target_pairs={{0,3},{1,0},{2,1},{3,2},{4,7},{5,4},{6,5},{7,6},{8,11},{9,8},{10,9... | collective-permute-start | bytes 3145736 | tf_op jit(solution)/shard_map/ppermute | solution.py:381
  13.9 0.5 collective-permute-start.11
  14.4 1.0 collective-permute-start.10
  15.5 1.4 %collective-permute-done.came_ref = bf16[40,256]{1,0:T(8,128)(2,1)S(1)} collective-permute-done((bf16[40,256]{1,0:T(8,128)(2,1)}, bf16[40,256]{1,0:T(8,128)(2,1)S(1)}, u32[]{:S(2)}, u32[]{:S(2)}) %collective-permute-start) | collective-permute-done | bytes 20512 | tf_op jit(solution)/shard_map/ppermute | solution.py:370
  16.9 0.7 copy-done.7
  17.7 0.7 collective-permute-start.5
  18.4 12.6 %collective-permute-start.4 = (bf16[40,256]{1,0:T(8,128)(2,1)S(1)}, bf16[40,256]{1,0:T(8,128)(2,1)S(1)}, u32[]{:S(2)}, u32[]{:S(2)}) collective-permute-start(bf16[40,256]{1,0:T(8,128)(2,1)S(1)} %shard_map.138), channel_id=1, source_target_pairs={{0,32},{24,56},{32,64},{56,88},{64,96},{88,120},{36,4},{60,28},{68... | collective-permute-start | bytes 61448 | tf_op jit(solution)/shard_map/ppermute | solution.py:375
  31.0 19.7 %collective-permute-start.3 = (bf16[40,256]{1,0:T(8,128)(2,1)S(1)}, bf16[40,256]{1,0:T(8,128)(2,1)S(1)}, u32[]{:S(2)}, u32[]{:S(2)}) collective-permute-start(bf16[40,256]{1,0:T(8,128)(2,1)S(1)} %shard_map.138), channel_id=1, source_target_pairs={{0,24},{8,32},{24,48},{32,56},{40,64},{56,80},{64,88},{72,96},{88,... | collective-permute-start | bytes 61448 | tf_op jit(solution)/shard_map/ppermute | solution.py:375
  50.6 4.9 %shard_map.136 = (f32[256,256]{1,0:T(8,128)}, f32[256,256]{1,0:T(8,128)}) custom-call(bf16[256,128]{1,0:T(8,128)(2,1)} %q_ref.3, bf16[256,128]{1,0:T(8,128)(2,1)} %k_ref.3, bf16[256,256]{1,0:T(8,128)(2,1)} %v_ref.3, f32[2,256,128]{2,1,0:T(8,128)} %d_ref.3, s32[1,256]{1,0:T(1,128)} %bitcast.5, bf16[256,256]{1,0:T(8,128)(2,1)} %gate_ref.1, f32[1,256]{1,0:T(1,128)} %bitcast.6), custom_call_target="tpu_custom_call" | custom-call | flops 536870912 | bytes 1048576 | tf_op jit(solution)/shard_map/pallas_call | solution.py:210
  55.5 1.3 collective-permute-start.2
  56.8 3.1 %collective-permute-start.1 = (bf16[40,256]{1,0:T(8,128)(2,1)S(1)}, bf16[40,256]{1,0:T(8,128)(2,1)S(1)}, u32[]{:S(2)}, u32[]{:S(2)}) collective-permute-start(bf16[40,256]{1,0:T(8,128)(2,1)S(1)} %shard_map.138), channel_id=1, source_target_pairs={{0,8},{8,16},{16,24},{24,32},{32,40},{40,48},{48,56},{56,64},{64,7... | collective-permute-start | bytes 61448 | tf_op jit(solution)/shard_map/ppermute | solution.py:375
  60.0 1.0 constant_dynamic-slice_fusion
  61.0 2.4 %collective-permute-start.15 = (bf16[64,512]{1,0:T(8,128)(2,1)S(1)}, bf16[64,512]{1,0:T(8,128)(2,1)S(1)}, u32[]{:S(2)}, u32[]{:S(2)}) collective-permute-start(bf16[64,512]{1,0:T(8,128)(2,1)S(1)} %get-tuple-element.55), channel_id=1, source_target_pairs={{0,3},{1,0},{2,1},{3,2},{4,7},{5,4},{6,5},{7,6},{8,11},{9,8},{10,9... | collective-permute-start | bytes 196616 | tf_op jit(solution)/shard_map/ppermute | solution.py:381
  63.3 0.7 copy-done.8
  64.3 0.6 copy-done.6
  64.9 1.2 collective-permute-done.6.other_ref
  66.1 1.8 %collective-permute-start.14 = (bf16[64,512]{1,0:T(8,128)(2,1)S(1)}, bf16[64,512]{1,0:T(8,128)(2,1)S(1)}, u32[]{:S(2)}, u32[]{:S(2)}) collective-permute-start(bf16[64,512]{1,0:T(8,128)(2,1)S(1)} %get-tuple-element.56), channel_id=1, source_target_pairs={{0,2},{1,3},{2,0},{3,1},{4,6},{5,7},{6,4},{7,5},{8,10},{9,11},{10,... | collective-permute-start | bytes 196616 | tf_op jit(solution)/shard_map/ppermute | solution.py:381
  67.8 2.3 %shard_map.140 = (bf16[64,256]{1,0:T(8,128)(2,1)}, bf16[64,256]{1,0:T(8,128)(2,1)}, bf16[64,256]{1,0:T(8,128)(2,1)}, bf16[64,256]{1,0:T(8,128)(2,1)}) custom-call(f32[256,256]{1,0:T(8,128)} %get-tuple-element.30.near_ref, f32[256,256]{1,0:T(8,128)} %get-tuple-element.31.factor_ref, bf16[256,128]{1,0:T(8,128)(2,1)} %get-tuple-element.32.qf_ref, ...), custom_call_target="tpu_custom_call" | custom-call | flops 67108864 | bytes 1048576 | tf_op jit(solution)/shard_map/pallas_call | solution.py:210
  70.1 2.4 %collective-permute-done.14.refs_10_ = bf16[64,512]{1,0:T(8,128)(2,1)S(1)} collective-permute-done((bf16[64,512]{1,0:T(8,128)(2,1)S(1)}, bf16[64,512]{1,0:T(8,128)(2,1)S(1)}, u32[]{:S(2)}, u32[]{:S(2)}) %collective-permute-start.14) | collective-permute-done | bytes 65568 | tf_op jit(solution)/shard_map/ppermute | solution.py:381
  72.5 0.9 collective-permute-done.13.refs_9_
  73.4 1.5 %collective-permute-start.8 = (bf16[64,256]{1,0:T(8,128)(2,1)}, bf16[64,256]{1,0:T(8,128)(2,1)S(1)}, u32[]{:S(2)}, u32[]{:S(2)}) collective-permute-start(bf16[64,256]{1,0:T(8,128)(2,1)} %get-tuple-element.41), channel_id=1, source_target_pairs={{0,2},{1,3},{2,0},{3,1},{4,6},{5,7},{6,4},{7,5},{8,10},{9,11},{10,... | collective-permute-start | bytes 98312 | tf_op jit(solution)/shard_map/ppermute | solution.py:381
  75.0 3.0 %collective-permute-done.7.refs_1_ = bf16[64,256]{1,0:T(8,128)(2,1)S(1)} collective-permute-done((bf16[64,256]{1,0:T(8,128)(2,1)}, bf16[64,256]{1,0:T(8,128)(2,1)S(1)}, u32[]{:S(2)}, u32[]{:S(2)}) %collective-permute-start.7) | collective-permute-done | bytes 32800 | tf_op jit(solution)/shard_map/ppermute | solution.py:381
  78.0 1.1 collective-permute-done.8.refs_2_
  79.1 3.0 %collective-permute-done.9.refs_3_ = bf16[64,256]{1,0:T(8,128)(2,1)S(1)} collective-permute-done((bf16[64,256]{1,0:T(8,128)(2,1)}, bf16[64,256]{1,0:T(8,128)(2,1)S(1)}, u32[]{:S(2)}, u32[]{:S(2)}) %collective-permute-start.9) | collective-permute-done | bytes 32800 | tf_op jit(solution)/shard_map/ppermute | solution.py:381
  82.1 1.3 copy-done
  83.4 0.7 copy-done.1
  84.1 0.7 copy-done.3
  84.8 0.8 copy-done.5
  85.6 2.7 %shard_map.141 = (f32[64,2048]{1,0:T(8,128)S(1)}, bf16[64,2048]{1,0:T(8,128)(2,1)S(1)}) custom-call(bf16[64,256]{1,0:T(8,128)(2,1)S(1)} %copy-done.5, bf16[64,256]{1,0:T(8,128)(2,1)S(1)} %collective-permute-done.7.refs_1_, bf16[64,256]{1,0:T(8,128)(2,1)S(1)} %collective-permute-done.8.refs_2_, bf16[64,256]{1,0:T(8,128)(2,1)S(1)} %collective-permute-done.9.refs_3_, ...), custom_call_target="tpu_custom_call" | custom-call | flops 268435456 | bytes 1048576 | tf_op jit(solution)/shard_map/pallas_call | solution.py:210
  88.4 3.2 %collective-permute-start.17 = (bf16[64,2048]{1,0:T(8,128)(2,1)S(1)}, bf16[64,2048]{1,0:T(8,128)(2,1)S(1)}, u32[]{:S(2)}, u32[]{:S(2)}) collective-permute-start(bf16[64,2048]{1,0:T(8,128)(2,1)S(1)} %get-tuple-element.46.refs_0_), channel_id=1, source_target_pairs={{0,3},{1,0},{2,1},{3,2},{4,7},{5,4},{6,5},{7,6},{8,11},{9,8},{10,9... | collective-permute-start | bytes 786440 | tf_op jit(solution)/shard_map/ppermute | solution.py:381
  91.6 9.3 %collective-permute-done.18.refs_2_ = bf16[64,2048]{1,0:T(8,128)(2,1)S(1)} collective-permute-done((bf16[64,2048]{1,0:T(8,128)(2,1)S(1)}, bf16[64,2048]{1,0:T(8,128)(2,1)S(1)}, u32[]{:S(2)}, u32[]{:S(2)}) %collective-permute-start.18) | collective-permute-done | bytes 262176 | tf_op jit(solution)/shard_map/ppermute | solution.py:381
  100.9 0.6 all-gather.2.cloned.1.call-done.refs_3_
  101.5 5.1 %shard_map.142 = (bf16[64,2048]{1,0:T(8,128)(2,1)S(1)}, bf16[64,2048]{1,0:T(8,128)(2,1)S(1)}, bf16[64,2048]{1,0:T(8,128)(2,1)S(1)}, bf16[2048,2304]{1,0:T(8,128)(2,1)S(1)}) custom-call(bf16[64,2048]{1,0:T(8,128)(2,1)S(1)} %collective-permute-done.16.refs_0_, bf16[64,2048]{1,0:T(8,128)(2,1)S(1)} %collective-permute-done.17.refs_1_, ...), custom_call_target="tpu_custom_call" | custom-call | flops 1811939328 | bytes 1048576 | tf_op jit(solution)/shard_map/pallas_call | solution.py:210
  106.6 1.3 collective-permute-start.19
  107.9 2.6 %collective-permute-start.20 = (bf16[64,2048]{1,0:T(8,128)(2,1)S(1)}, bf16[64,2048]{1,0:T(8,128)(2,1)S(1)}, u32[]{:S(2)}, u32[]{:S(2)}) collective-permute-start(bf16[64,2048]{1,0:T(8,128)(2,1)S(1)} %get-tuple-element.49), channel_id=1, source_target_pairs={{0,2},{1,3},{2,0},{3,1},{4,6},{5,7},{6,4},{7,5},{8,10},{9,11},{10,... | collective-permute-start | bytes 786440 | tf_op jit(solution)/shard_map/ppermute | solution.py:414
  110.6 1.6 %collective-permute-start.21 = (bf16[64,2048]{1,0:T(8,128)(2,1)S(1)}, bf16[64,2048]{1,0:T(8,128)(2,1)S(1)}, u32[]{:S(2)}, u32[]{:S(2)}) collective-permute-start(bf16[64,2048]{1,0:T(8,128)(2,1)S(1)} %get-tuple-element.50), channel_id=1, source_target_pairs={{0,3},{1,0},{2,1},{3,2},{4,7},{5,4},{6,5},{7,6},{8,11},{9,8},{10,9... | collective-permute-start | bytes 786440 | tf_op jit(solution)/shard_map/ppermute | solution.py:414
  112.1 2.1 %shard_map.143.refs_0_ = bf16[64,2048]{1,0:T(8,128)(2,1)S(1)} custom-call(bf16[64,2048]{1,0:T(8,128)(2,1)S(1)} %get-tuple-element.46.refs_0_, bf16[2048,2304]{1,0:T(8,128)(2,1)S(1)} %get-tuple-element.47.refs_1_), custom_call_target="tpu_custom_call" | custom-call | flops 603979776 | bytes 1048576 | tf_op jit(solution)/shard_map/pallas_call | solution.py:210
  114.2 2.3 %collective-permute-done.19.refs_1_ = bf16[64,2048]{1,0:T(8,128)(2,1)S(1)} collective-permute-done((bf16[64,2048]{1,0:T(8,128)(2,1)S(1)}, bf16[64,2048]{1,0:T(8,128)(2,1)S(1)}, u32[]{:S(2)}, u32[]{:S(2)}) %collective-permute-start.19) | collective-permute-done | bytes 262176 | tf_op jit(solution)/shard_map/ppermute | solution.py:414
  116.5 6.1 %collective-permute-done.20.refs_2_ = bf16[64,2048]{1,0:T(8,128)(2,1)S(1)} collective-permute-done((bf16[64,2048]{1,0:T(8,128)(2,1)S(1)}, bf16[64,2048]{1,0:T(8,128)(2,1)S(1)}, u32[]{:S(2)}, u32[]{:S(2)}) %collective-permute-start.20) | collective-permute-done | bytes 262176 | tf_op jit(solution)/shard_map/ppermute | solution.py:414
  122.6 0.4 shard_map.144
  123.0 1.8 %collective-permute-start.22 = (bf16[64,512]{1,0:T(8,128)(2,1)S(1)}, bf16[64,512]{1,0:T(8,128)(2,1)S(1)}, u32[]{:S(2)}, u32[]{:S(2)}) collective-permute-start(bf16[64,512]{1,0:T(8,128)(2,1)S(1)} %get-tuple-element.52), channel_id=1, source_target_pairs={{0,1},{1,2},{2,3},{3,0},{4,5},{5,6},{6,7},{7,4},{8,9},{9,10},{10,1... | collective-permute-start | bytes 196616 | tf_op jit(solution)/shard_map/ppermute | solution.py:381
  124.8 2.4 %collective-permute-start.23 = (bf16[64,512]{1,0:T(8,128)(2,1)S(1)}, bf16[64,512]{1,0:T(8,128)(2,1)S(1)}, u32[]{:S(2)}, u32[]{:S(2)}) collective-permute-start(bf16[64,512]{1,0:T(8,128)(2,1)S(1)} %get-tuple-element.53), channel_id=1, source_target_pairs={{0,2},{1,3},{2,0},{3,1},{4,6},{5,7},{6,4},{7,5},{8,10},{9,11},{10,... | collective-permute-start | bytes 196616 | tf_op jit(solution)/shard_map/ppermute | solution.py:381
  127.2 1.3 collective-permute-start.24
  128.6 2.0 %collective-permute-done.23.refs_2_ = bf16[64,512]{1,0:T(8,128)(2,1)S(1)} collective-permute-done((bf16[64,512]{1,0:T(8,128)(2,1)S(1)}, bf16[64,512]{1,0:T(8,128)(2,1)S(1)}, u32[]{:S(2)}, u32[]{:S(2)}) %collective-permute-start.23) | collective-permute-done | bytes 65568 | tf_op jit(solution)/shard_map/ppermute | solution.py:381
  130.6 0.9 collective-permute-done.24.refs_3_
  131.5 0.7 shard_map.145
  (37 shorter events, 0.7 us)
Async XLA Ops:
  6.5 95.0 %all-gather.2.cloned.1.call-start = ((), (), s32[]{:S(2)}) async-start(), calls=%async_computation | async-start | bytes 9732096 | tf_op jit(solution)/shard_map/all_gather | solution.py:396
  10.7 71.4 %collective-permute-start.12 = (bf16[256,2048]{1,0:T(8,128)(2,1)}, bf16[256,2048]{1,0:T(8,128)(2,1)S(1)}, u32[]{:S(2)}, u32[]{:S(2)}) collective-permute-start(bf16[256,2048]{1,0:T(8,128)(2,1)} %refs_4_.1), channel_id=1, source_target_pairs={{0,3},{1,0},{2,1},{3,2},{4,7},{5,4},{6,5},{7,6},{8,11},{9,8},{10,9... | collective-permute-start | bytes 3145736 | tf_op jit(solution)/shard_map/ppermute | solution.py:381
  13.9 68.2 %collective-permute-start.11 = (bf16[256,2048]{1,0:T(8,128)(2,1)}, bf16[256,2048]{1,0:T(8,128)(2,1)}, u32[]{:S(2)}, u32[]{:S(2)}) collective-permute-start(bf16[256,2048]{1,0:T(8,128)(2,1)} %refs_4_.1), channel_id=1, source_target_pairs={{0,2},{1,3},{2,0},{3,1},{4,6},{5,7},{6,4},{7,5},{8,10},{9,11},{10,... | collective-permute-start | bytes 3145736 | tf_op jit(solution)/shard_map/ppermute | solution.py:381
  14.4 67.7 %collective-permute-start.10 = (bf16[256,2048]{1,0:T(8,128)(2,1)}, bf16[256,2048]{1,0:T(8,128)(2,1)}, u32[]{:S(2)}, u32[]{:S(2)}) collective-permute-start(bf16[256,2048]{1,0:T(8,128)(2,1)} %refs_4_.1), channel_id=1, source_target_pairs={{0,1},{1,2},{2,3},{3,0},{4,5},{5,6},{6,7},{7,4},{8,9},{9,10},{10,1... | collective-permute-start | bytes 3145736 | tf_op jit(solution)/shard_map/ppermute | solution.py:381
  15.5 1.4 %collective-permute-start = (bf16[40,256]{1,0:T(8,128)(2,1)}, bf16[40,256]{1,0:T(8,128)(2,1)S(1)}, u32[]{:S(2)}, u32[]{:S(2)}) collective-permute-start(bf16[40,256]{1,0:T(8,128)(2,1)} %get-tuple-element.36), channel_id=1, source_target_pairs={{0,4},{4,0},{8,12},{12,8},{16,20},{20,16},{24,28},{28,24},{32,36},... | collective-permute-start | bytes 61448 | tf_op jit(solution)/shard_map/ppermute | solution.py:370
  16.9 0.7 copy-start.7
  17.7 13.2 %collective-permute-start.5 = (bf16[40,256]{1,0:T(8,128)(2,1)S(1)}, bf16[40,256]{1,0:T(8,128)(2,1)S(1)}, u32[]{:S(2)}, u32[]{:S(2)}) collective-permute-start(bf16[40,256]{1,0:T(8,128)(2,1)S(1)} %shard_map.138), channel_id=1, source_target_pairs={{24,64},{56,96},{68,28},{100,60},{25,65},{57,97},{69,29},{101,61},... | collective-permute-start | bytes 61448 | tf_op jit(solution)/shard_map/ppermute | solution.py:375
  18.4 37.2 %collective-permute-start.4 = (bf16[40,256]{1,0:T(8,128)(2,1)S(1)}, bf16[40,256]{1,0:T(8,128)(2,1)S(1)}, u32[]{:S(2)}, u32[]{:S(2)}) collective-permute-start(bf16[40,256]{1,0:T(8,128)(2,1)S(1)} %shard_map.138), channel_id=1, source_target_pairs={{0,32},{24,56},{32,64},{56,88},{64,96},{88,120},{36,4},{60,28},{68... | collective-permute-start | bytes 61448 | tf_op jit(solution)/shard_map/ppermute | solution.py:375
  31.0 25.9 %collective-permute-start.3 = (bf16[40,256]{1,0:T(8,128)(2,1)S(1)}, bf16[40,256]{1,0:T(8,128)(2,1)S(1)}, u32[]{:S(2)}, u32[]{:S(2)}) collective-permute-start(bf16[40,256]{1,0:T(8,128)(2,1)S(1)} %shard_map.138), channel_id=1, source_target_pairs={{0,24},{8,32},{24,48},{32,56},{40,64},{56,80},{64,88},{72,96},{88,... | collective-permute-start | bytes 61448 | tf_op jit(solution)/shard_map/ppermute | solution.py:375
  55.5 5.4 %collective-permute-start.2 = (bf16[40,256]{1,0:T(8,128)(2,1)S(1)}, bf16[40,256]{1,0:T(8,128)(2,1)S(1)}, u32[]{:S(2)}, u32[]{:S(2)}) collective-permute-start(bf16[40,256]{1,0:T(8,128)(2,1)S(1)} %shard_map.138), channel_id=1, source_target_pairs={{0,16},{8,24},{16,32},{24,40},{32,48},{40,56},{48,64},{56,72},{64,... | collective-permute-start | bytes 61448 | tf_op jit(solution)/shard_map/ppermute | solution.py:375
  56.8 6.5 %collective-permute-start.1 = (bf16[40,256]{1,0:T(8,128)(2,1)S(1)}, bf16[40,256]{1,0:T(8,128)(2,1)S(1)}, u32[]{:S(2)}, u32[]{:S(2)}) collective-permute-start(bf16[40,256]{1,0:T(8,128)(2,1)S(1)} %shard_map.138), channel_id=1, source_target_pairs={{0,8},{8,16},{16,24},{24,32},{32,40},{40,48},{48,56},{56,64},{64,7... | collective-permute-start | bytes 61448 | tf_op jit(solution)/shard_map/ppermute | solution.py:375
  61.0 6.8 %collective-permute-start.15 = (bf16[64,512]{1,0:T(8,128)(2,1)S(1)}, bf16[64,512]{1,0:T(8,128)(2,1)S(1)}, u32[]{:S(2)}, u32[]{:S(2)}) collective-permute-start(bf16[64,512]{1,0:T(8,128)(2,1)S(1)} %get-tuple-element.55), channel_id=1, source_target_pairs={{0,3},{1,0},{2,1},{3,2},{4,7},{5,4},{6,5},{7,6},{8,11},{9,8},{10,9... | collective-permute-start | bytes 196616 | tf_op jit(solution)/shard_map/ppermute | solution.py:381
  63.3 0.7 copy-start.8
  64.3 0.6 copy-start.6
  64.9 1.2 collective-permute-start.6
  66.1 1.8 %copy-start.9 = (bf16[40,256]{1,0:T(8,128)(2,1)}, bf16[40,256]{1,0:T(8,128)(2,1)S(1)}, u32[]{:S(2)}) copy-start(bf16[40,256]{1,0:T(8,128)(2,1)S(1)} %collective-permute-done.6.other_ref) | copy-start | bytes 61444
  66.1 6.5 %collective-permute-start.14 = (bf16[64,512]{1,0:T(8,128)(2,1)S(1)}, bf16[64,512]{1,0:T(8,128)(2,1)S(1)}, u32[]{:S(2)}, u32[]{:S(2)}) collective-permute-start(bf16[64,512]{1,0:T(8,128)(2,1)S(1)} %get-tuple-element.56), channel_id=1, source_target_pairs={{0,2},{1,3},{2,0},{3,1},{4,6},{5,7},{6,4},{7,5},{8,10},{9,11},{10,... | collective-permute-start | bytes 196616 | tf_op jit(solution)/shard_map/ppermute | solution.py:381
  67.8 5.6 %collective-permute-start.13 = (bf16[64,512]{1,0:T(8,128)(2,1)S(1)}, bf16[64,512]{1,0:T(8,128)(2,1)S(1)}, u32[]{:S(2)}, u32[]{:S(2)}) collective-permute-start(bf16[64,512]{1,0:T(8,128)(2,1)S(1)} %get-tuple-element.57), channel_id=1, source_target_pairs={{0,1},{1,2},{2,3},{3,0},{4,5},{5,6},{6,7},{7,4},{8,9},{9,10},{10,1... | collective-permute-start | bytes 196616 | tf_op jit(solution)/shard_map/ppermute | solution.py:381
  72.5 5.4 %collective-permute-start.7 = (bf16[64,256]{1,0:T(8,128)(2,1)}, bf16[64,256]{1,0:T(8,128)(2,1)S(1)}, u32[]{:S(2)}, u32[]{:S(2)}) collective-permute-start(bf16[64,256]{1,0:T(8,128)(2,1)} %get-tuple-element.40), channel_id=1, source_target_pairs={{0,1},{1,2},{2,3},{3,0},{4,5},{5,6},{6,7},{7,4},{8,9},{9,10},{10,1... | collective-permute-start | bytes 98312 | tf_op jit(solution)/shard_map/ppermute | solution.py:381
  73.4 5.6 %collective-permute-start.8 = (bf16[64,256]{1,0:T(8,128)(2,1)}, bf16[64,256]{1,0:T(8,128)(2,1)S(1)}, u32[]{:S(2)}, u32[]{:S(2)}) collective-permute-start(bf16[64,256]{1,0:T(8,128)(2,1)} %get-tuple-element.41), channel_id=1, source_target_pairs={{0,2},{1,3},{2,0},{3,1},{4,6},{5,7},{6,4},{7,5},{8,10},{9,11},{10,... | collective-permute-start | bytes 98312 | tf_op jit(solution)/shard_map/ppermute | solution.py:381
  78.0 4.1 %collective-permute-start.9 = (bf16[64,256]{1,0:T(8,128)(2,1)}, bf16[64,256]{1,0:T(8,128)(2,1)S(1)}, u32[]{:S(2)}, u32[]{:S(2)}) collective-permute-start(bf16[64,256]{1,0:T(8,128)(2,1)} %get-tuple-element.42), channel_id=1, source_target_pairs={{0,3},{1,0},{2,1},{3,2},{4,7},{5,4},{6,5},{7,6},{8,11},{9,8},{10,9... | collective-permute-start | bytes 98312 | tf_op jit(solution)/shard_map/ppermute | solution.py:381
  82.1 1.3 copy-start
  83.4 0.7 copy-start.1
  84.1 0.7 copy-start.3
  84.8 0.8 copy-start.5
  88.3 34.4 %copy-start.2 = (f32[2,2048]{1,0:T(2,128)S(1)}, f32[2,2048]{1,0:T(2,128)}, u32[]{:S(2)}) copy-start(f32[2,2048]{1,0:T(2,128)} %refs_4_.2) | copy-start | bytes 49156
  88.3 34.3 %copy-start.4 = (f32[2,2048]{1,0:T(2,128)S(1)}, f32[2,2048]{1,0:T(2,128)}, u32[]{:S(2)}) copy-start(f32[2,2048]{1,0:T(2,128)} %refs_5_.1) | copy-start | bytes 49156
  88.3 12.6 %collective-permute-start.18 = (bf16[64,2048]{1,0:T(8,128)(2,1)S(1)}, bf16[64,2048]{1,0:T(8,128)(2,1)S(1)}, u32[]{:S(2)}, u32[]{:S(2)}) collective-permute-start(bf16[64,2048]{1,0:T(8,128)(2,1)S(1)} %get-tuple-element.46.refs_0_), channel_id=1, source_target_pairs={{0,1},{1,2},{2,3},{3,0},{4,5},{5,6},{6,7},{7,4},{8,9},{9,10},{10,1... | collective-permute-start | bytes 786440 | tf_op jit(solution)/shard_map/ppermute | solution.py:381
  88.4 12.5 %collective-permute-start.17 = (bf16[64,2048]{1,0:T(8,128)(2,1)S(1)}, bf16[64,2048]{1,0:T(8,128)(2,1)S(1)}, u32[]{:S(2)}, u32[]{:S(2)}) collective-permute-start(bf16[64,2048]{1,0:T(8,128)(2,1)S(1)} %get-tuple-element.46.refs_0_), channel_id=1, source_target_pairs={{0,3},{1,0},{2,1},{3,2},{4,7},{5,4},{6,5},{7,6},{8,11},{9,8},{10,9... | collective-permute-start | bytes 786440 | tf_op jit(solution)/shard_map/ppermute | solution.py:381
  91.6 9.3 %collective-permute-start.16 = (bf16[64,2048]{1,0:T(8,128)(2,1)S(1)}, bf16[64,2048]{1,0:T(8,128)(2,1)S(1)}, u32[]{:S(2)}, u32[]{:S(2)}) collective-permute-start(bf16[64,2048]{1,0:T(8,128)(2,1)S(1)} %get-tuple-element.46.refs_0_), channel_id=1, source_target_pairs={{0,2},{1,3},{2,0},{3,1},{4,6},{5,7},{6,4},{7,5},{8,10},{9,11},{10,... | collective-permute-start | bytes 786440 | tf_op jit(solution)/shard_map/ppermute | solution.py:381
  106.6 9.9 %collective-permute-start.19 = (bf16[64,2048]{1,0:T(8,128)(2,1)S(1)}, bf16[64,2048]{1,0:T(8,128)(2,1)S(1)}, u32[]{:S(2)}, u32[]{:S(2)}) collective-permute-start(bf16[64,2048]{1,0:T(8,128)(2,1)S(1)} %get-tuple-element.48), channel_id=1, source_target_pairs={{0,1},{1,2},{2,3},{3,0},{4,5},{5,6},{6,7},{7,4},{8,9},{9,10},{10,1... | collective-permute-start | bytes 786440 | tf_op jit(solution)/shard_map/ppermute | solution.py:414
  107.9 14.7 %collective-permute-start.20 = (bf16[64,2048]{1,0:T(8,128)(2,1)S(1)}, bf16[64,2048]{1,0:T(8,128)(2,1)S(1)}, u32[]{:S(2)}, u32[]{:S(2)}) collective-permute-start(bf16[64,2048]{1,0:T(8,128)(2,1)S(1)} %get-tuple-element.49), channel_id=1, source_target_pairs={{0,2},{1,3},{2,0},{3,1},{4,6},{5,7},{6,4},{7,5},{8,10},{9,11},{10,... | collective-permute-start | bytes 786440 | tf_op jit(solution)/shard_map/ppermute | solution.py:414
  110.6 12.0 %collective-permute-start.21 = (bf16[64,2048]{1,0:T(8,128)(2,1)S(1)}, bf16[64,2048]{1,0:T(8,128)(2,1)S(1)}, u32[]{:S(2)}, u32[]{:S(2)}) collective-permute-start(bf16[64,2048]{1,0:T(8,128)(2,1)S(1)} %get-tuple-element.50), channel_id=1, source_target_pairs={{0,3},{1,0},{2,1},{3,2},{4,7},{5,4},{6,5},{7,6},{8,11},{9,8},{10,9... | collective-permute-start | bytes 786440 | tf_op jit(solution)/shard_map/ppermute | solution.py:414
  123.0 5.6 %collective-permute-start.22 = (bf16[64,512]{1,0:T(8,128)(2,1)S(1)}, bf16[64,512]{1,0:T(8,128)(2,1)S(1)}, u32[]{:S(2)}, u32[]{:S(2)}) collective-permute-start(bf16[64,512]{1,0:T(8,128)(2,1)S(1)} %get-tuple-element.52), channel_id=1, source_target_pairs={{0,1},{1,2},{2,3},{3,0},{4,5},{5,6},{6,7},{7,4},{8,9},{9,10},{10,1... | collective-permute-start | bytes 196616 | tf_op jit(solution)/shard_map/ppermute | solution.py:381
  124.8 5.8 %collective-permute-start.23 = (bf16[64,512]{1,0:T(8,128)(2,1)S(1)}, bf16[64,512]{1,0:T(8,128)(2,1)S(1)}, u32[]{:S(2)}, u32[]{:S(2)}) collective-permute-start(bf16[64,512]{1,0:T(8,128)(2,1)S(1)} %get-tuple-element.53), channel_id=1, source_target_pairs={{0,2},{1,3},{2,0},{3,1},{4,6},{5,7},{6,4},{7,5},{8,10},{9,11},{10,... | collective-permute-start | bytes 196616 | tf_op jit(solution)/shard_map/ppermute | solution.py:381
  127.2 4.3 %collective-permute-start.24 = (bf16[64,512]{1,0:T(8,128)(2,1)S(1)}, bf16[64,512]{1,0:T(8,128)(2,1)S(1)}, u32[]{:S(2)}, u32[]{:S(2)}) collective-permute-start(bf16[64,512]{1,0:T(8,128)(2,1)S(1)} %get-tuple-element.54), channel_id=1, source_target_pairs={{0,3},{1,0},{2,1},{3,2},{4,7},{5,4},{6,5},{7,6},{8,11},{9,8},{10,9... | collective-permute-start | bytes 196616 | tf_op jit(solution)/shard_map/ppermute | solution.py:381
Sparse Core Ops, SparseCore 0:
  9.2 92.2 all-gather.1
